TPU v7x, 32 devices: a whole 2x2x4 slice. The times are simulated.
32 devices in a mesh: kv: 8 (over z, x), tp: 4 (over y, core).
Axes of the slice: x: 2, y: 2, z: 4, core: 2. Of those that a mesh axis runs over, the one named last changes fastest.
Arguments:
- queries: bfloat16 [64, 4, 8, 128], P('kv', None, 'tp'), may hold values from -6 to 6
- keys: bfloat16 [64, 4, 8, 128], P('kv', None, 'tp'), may hold values from -6 to 6
- values: bfloat16 [64, 4, 8, 256], P('kv', None, 'tp'), may hold values from -6 to 6
- in_gate: float32 [64, 4, 8], P('kv', None, 'tp'), may hold values from -6 to 6
- forget_pre: float32 [64, 4, 8], P('kv', None, 'tp'), may hold values from -1 to 5
- old_keys: bfloat16 [64, 4, 8, 128], P('kv', None, 'tp'), may hold values from -6 to 6
- old_values: bfloat16 [64, 4, 8, 256], P('kv', None, 'tp'), may hold values from -6 to 6
- old_in_gate: float32 [64, 4, 8], P('kv', None, 'tp'), may hold values from -6 to 6
- old_forget: float32 [64, 4, 8], P('kv', None, 'tp'), may hold values from -1 to 5
- accepted: int32 [64], P('kv'), may hold values from 0 to 4
- state_mem: float32 [64, 8, 128, 256], P('kv', 'tp'), may hold values from -4 to 4
- state_norm: float32 [64, 8, 128], P('kv', 'tp'), may hold values from -6 to 6
- state_max: float32 [64, 8], P('kv', 'tp'), may hold values from -4 to 4
- norm_gain: float32 [8, 256], P('tp'), may hold values from 0.1 to 1.9
- out_weight: bfloat16 [2048, 2048], P('tp', 'kv'), may hold values from -0.125 to 0.125
Outputs:
- mixed: bfloat16 [64, 4, 2048], P('kv', 'tp')
- new_mem: float32 [64, 8, 128, 256], P('kv', 'tp')
- new_norm: float32 [64, 8, 128], P('kv', 'tp')
- new_max: float32 [64, 8], P('kv', 'tp')
Inputs may be any that keep to these rules, and one draw needn't show every extreme that they name: How many of the last step's 4 proposals of a sequence were accepted.
All inputs are finite; a program needn't handle non-finite values.
Results may differ from a plain program's by a relative error of at most 0.0068.
Values may be sent and summed in bfloat16 or wider, within the bound.
A program may use at most 64 MiB of HBM per device.

v0:
```python
import jax
import jax.numpy as jnp
from jax import lax
from jax.sharding import PartitionSpec as P

HIGH = lax.Precision.HIGHEST


def cell(queries, keys, values, in_gates, log_forget, memory, normal, stab):
    length = in_gates.shape[-1]
    causal = jnp.tril(jnp.ones((length, length), dtype=bool))
    cumul = jnp.cumsum(log_forget, axis=-1)
    logd = jnp.where(causal, cumul[:, :, None] - cumul[:, None, :] + in_gates[:, None, :], -jnp.inf)
    inter = cumul + stab[:, None]
    m_row = jnp.maximum(inter, jnp.max(logd, axis=-1))
    scores = jnp.einsum("hld,hsd->hls", queries, keys, precision=HIGH) * jnp.exp(
        logd - m_row[..., None]
    )
    w_inter = jnp.exp(inter - m_row)
    num = w_inter[..., None] * jnp.einsum(
        "hld,hde->hle", queries, memory, precision=HIGH
    ) + jnp.einsum("hls,hse->hle", scores, values, precision=HIGH)
    den = w_inter * jnp.einsum("hld,hd->hl", queries, normal, precision=HIGH) + jnp.sum(
        scores, axis=-1
    )
    hidden = num / jnp.maximum(jnp.abs(den), 1.0)[..., None]
    m_new = m_row[:, -1]
    g_state = jnp.exp(cumul[:, -1] + stab - m_new)
    g_tok = jnp.exp(cumul[:, -1:] - cumul + in_gates - m_new[:, None])
    mem_new = g_state[:, None, None] * memory + jnp.einsum(
        "hld,hle->hde", g_tok[..., None] * keys, values, precision=HIGH
    )
    norm_new = g_state[:, None] * normal + jnp.einsum("hl,hld->hd", g_tok, keys, precision=HIGH)
    return (hidden, mem_new, norm_new, m_new)


def one_sequence(
    queries,
    keys,
    values,
    in_gate,
    forget_pre,
    old_keys,
    old_values,
    old_in_gate,
    old_forget,
    accepted,
    memory,
    normal,
    stab,
    norm_gain,
):
    props = queries.shape[0]
    live = jnp.arange(props, dtype=jnp.int32) < accepted
    gates = jnp.concatenate([jnp.where(live[:, None], old_in_gate, -jnp.inf), in_gate], axis=0)
    forget = jnp.concatenate(
        [
            jnp.where(live[:, None], jax.nn.log_sigmoid(old_forget), 0.0),
            jax.nn.log_sigmoid(forget_pre),
        ],
        axis=0,
    )
    scale = queries.shape[-1] ** (-0.5)
    qrun = jnp.concatenate(
        [jnp.zeros(queries.shape, jnp.float32), queries.astype(jnp.float32) * scale], axis=0
    )
    krun = jnp.concatenate([old_keys, keys], axis=0).astype(jnp.float32)
    vrun = jnp.concatenate([old_values, values], axis=0).astype(jnp.float32)
    hidden, mem_new, norm_new, m_new = cell(
        jnp.swapaxes(qrun, 0, 1),
        jnp.swapaxes(krun, 0, 1),
        jnp.swapaxes(vrun, 0, 1),
        gates.T,
        forget.T,
        memory,
        normal,
        stab,
    )
    hidden = hidden[:, props:, :]
    mean = jnp.mean(hidden, -1, keepdims=True)
    var = jnp.mean(jnp.square(hidden - mean), -1, keepdims=True)
    normed = (hidden - mean) * lax.rsqrt(var + 1e-05) * norm_gain[:, None, :]
    flat = jnp.swapaxes(normed, 0, 1).reshape(props, -1).astype(jnp.bfloat16)
    return (flat, mem_new, norm_new, m_new)


def on_device(
    queries,
    keys,
    values,
    in_gate,
    forget_pre,
    old_keys,
    old_values,
    old_in_gate,
    old_forget,
    accepted,
    state_mem,
    state_norm,
    state_max,
    norm_gain,
    out_weight,
):
    mapped = jax.vmap(one_sequence, in_axes=(0, 0, 0, 0, 0, 0, 0, 0, 0, 0, 0, 0, 0, None))
    hidden, new_mem, new_norm, new_max = mapped(
        queries,
        keys,
        values,
        in_gate,
        forget_pre,
        old_keys,
        old_values,
        old_in_gate,
        old_forget,
        accepted,
        state_mem,
        state_norm,
        state_max,
        norm_gain,
    )
    terms = jnp.einsum(
        "spr,rc->spc",
        hidden,
        lax.all_gather(out_weight, "kv", axis=1, tiled=True),
        preferred_element_type=jnp.float32,
    )
    mixed = lax.psum_scatter(terms, "tp", scatter_dimension=1, tiled=True).astype(jnp.bfloat16)
    return (mixed, new_mem, new_norm, new_max)


def solution(mesh):
    return jax.shard_map(
        on_device,
        mesh=mesh,
        in_specs=(
            P("kv", None, "tp", None),
            P("kv", None, "tp", None),
            P("kv", None, "tp", None),
            P("kv", None, "tp"),
            P("kv", None, "tp"),
            P("kv", None, "tp", None),
            P("kv", None, "tp", None),
            P("kv", None, "tp"),
            P("kv", None, "tp"),
            P("kv"),
            P("kv", "tp", None, None),
            P("kv", "tp", None),
            P("kv", "tp"),
            P("tp", None),
            P("tp", "kv"),
        ),
        out_specs=(
            P("kv", "tp", None),
            P("kv", "tp", None, None),
            P("kv", "tp", None),
            P("kv", "tp"),
        ),
        check_vma=False,
    )
```

profile of v0, /device:TPU:0, one launch (start us, length us, event | category | flops | bytes accessed | tf_op | source)
XLA Modules:
  0.0 92.6 jit_solution(17613975096085614680)
XLA Ops:
  7.2 0.7 all-gather.2.cloned.1.call-update
  8.0 0.7 iota_compare_fusion.1
  8.6 0.7 fusion.19
  9.3 0.7 fusion.20
  10.1 0.7 copy.75
  10.9 0.1 copy.72
  10.9 0.1 fusion.5
  11.1 0.7 add_maximum_fusion
  11.8 0.1 copy.84
  11.9 0.7 copy.82
  12.7 0.7 copy.81
  13.4 0.7 convert_multiply_fusion
  14.1 0.2 fusion.27
  14.4 0.9 %fusion.7 = f32[8,2,1,8]{3,2,1,0:T(1,128)S(1)} fusion(f32[8,2,128,1]{2,3,1,0:T(1,128)} %bitcast.50, f32[8,2,8,128]{3,0,1,2:T(8,128)S(1)} %pad_bitcast_fusion), kind=kOutput, calls=%fused_computation.16 | convolution fusion | flops 196608 | bytes 74240 | tf_op jit(solution)/shard_map/vmap(hld,hd->hl)/dot_general | solution.py:23
  15.5 0.7 fusion.17
  16.2 0.1 copy.113
  16.3 0.8 copy.86
  17.0 0.8 copy.85
  17.8 0.1 copy.114
  17.9 0.3 fusion.11
  18.2 1.1 %fusion.9 = f32[8,2,8,256]{3,2,1,0:T(8,128)S(1)} fusion(f32[8,2,128,256]{3,2,1,0:T(8,128)S(1)} %copy-done, f32[8,2,8,128]{3,0,1,2:T(8,128)S(1)} %pad_bitcast_fusion), kind=kOutput, calls=%fused_computation.18 | convolution fusion | flops 50331648 | bytes 2293760 | tf_op jit(solution)/shard_map/vmap(hld,hde->hle)/dot_general | solution.py:20
  19.3 0.2 fusion.25
  19.5 0.2 multiply_reduce_fusion
  19.7 0.1 fusion.12
  19.9 0.1 copy.91
  20.2 0.2 fusion.14
  20.4 42.7 %all-gather.2.cloned.1.call-done = bf16[512,2048]{1,0:T(8,128)(2,1)} async-done(((bf16[512,256]{1,0:T(8,128)(2,1)}), bf16[512,2048]{1,0:T(8,128)(2,1)}) %all-gather.2.cloned.1.call-update) | async-done | bytes 2097168 | tf_op jit(solution)/shard_map/all_gather | solution.py:124
  63.1 2.8 %fusion = f32[8,4,2048]{2,0,1:T(8,128)} fusion(bf16[8,4,512]{2,0,1:T(8,128)(2,1)S(1)} %convert_element_type.20, bf16[512,2048]{1,0:T(8,128)(2,1)} %all-gather.2.cloned.1.call-done), kind=kOutput, calls=%fused_computation | convolution fusion | flops 67108864 | bytes 2392064 | tf_op jit(solution)/shard_map/spr,rc->spc/dot_general | solution.py:121
  65.9 0.7 multiply_add_fusion.1
  66.6 2.7 %multiply_add_fusion = f32[8,2,128,256]{3,2,1,0:T(8,128)} fusion(f32[8,2,128,256]{3,2,1,0:T(8,128)S(1)} %copy-done, f32[8,2]{1,0:T(8,128)S(1)} %copy.91, bf16[8,4,2,256]{3,1,2,0:T(4,128)(2,1)S(1)} %copy.86, bf16[8,4,2,256]{3,1,2,0:T(4,128)(2,1)S(1)} %copy.85, f32[8,2,8]{2,1,0:T(2,128)S(1)} %copy.92, bf16[8,4,2,128]{3,1,2,0:T(4,128)(2,1)S(1)} %copy.82, ...), kind=kOutput, calls=%fused_computation.2 | convolution fusion | flops 51609600 | bytes 4293184 | tf_op jit(solution)/shard_map/vmap(hld,hle->hde)/dot_general | solution.py:30
  69.3 15.0 %reduce-scatter.2.cloned.1.call-done = f32[8,1,2048]{2,0,1:T(8,128)} async-done(((f32[8,4,2048]{2,0,1:T(8,128)}), f32[8,1,2048]{2,0,1:T(8,128)}) %reduce-scatter.2.cloned.1.call-update) | async-done | bytes 65552 | tf_op jit(solution)/shard_map/reduce_scatter | solution.py:127
  84.3 1.5 %convert_element_type.21 = bf16[8,1,2048]{2,0,1:T(8,128)(2,1)} convert(f32[8,1,2048]{2,0,1:T(8,128)} %reduce-scatter.2.cloned.1.call-done) | non-fusion elementwise | flops 16384 | bytes 98304 | tf_op jit(solution)/shard_map/convert_element_type | solution.py:127
  (32 shorter events, 0.7 us)
Async XLA Ops:
  7.2 11.0 %copy-start = (f32[8,2,128,256]{3,2,1,0:T(8,128)S(1)}, f32[8,2,128,256]{3,2,1,0:T(8,128)}, u32[]{:S(2)}) copy-start(f32[8,2,128,256]{3,2,1,0:T(8,128)} %param.25) | copy-start | bytes 6291460
  7.2 55.9 %all-gather.2.cloned.1.call-start = ((), (), s32[]{:S(2)}) async-start(), calls=%async_computation.1 | async-start | bytes 2359296 | tf_op jit(solution)/shard_map/all_gather | solution.py:124
  7.9 76.4 %reduce-scatter.2.cloned.1.call-start = ((), (), s32[]{:S(2)}) async-start(), calls=%async_computation.2 | async-start | bytes 327680 | tf_op jit(solution)/shard_map/reduce_scatter | solution.py:127
  11.9 8.0 %copy-start.3 = (f32[8,2,1]{0,2,1:T(1,128)}, f32[8,2,1]{0,2,1:T(1,128)S(1)}, u32[]{:S(2)}) copy-start(f32[8,2,1]{0,2,1:T(1,128)S(1)} %slice.18) | copy-start | bytes 196
  14.1 5.6 %copy-start.4 = (f32[2,256]{1,0:T(2,128)S(1)}, f32[2,256]{1,0:T(2,128)}, u32[]{:S(2)}) copy-start(f32[2,256]{1,0:T(2,128)} %param.28) | copy-start | bytes 6148
  14.1 5.8 %copy-start.2 = (f32[8,2]{0,1:T(2,128)S(1)}, f32[8,2]{0,1:T(2,128)}, u32[]{:S(2)}) copy-start(f32[8,2]{0,1:T(2,128)} %param.27) | copy-start | bytes 196
  19.3 46.6 %copy-start.1 = (f32[8,2,128]{2,1,0:T(2,128)S(1)}, f32[8,2,128]{2,1,0:T(2,128)}, u32[]{:S(2)}) copy-start(f32[8,2,128]{2,1,0:T(2,128)} %param.26) | copy-start | bytes 24580
Sparse Core Ops, SparseCore 0:
  10.0 53.0 all-gather.1
  66.0 18.2 reduce-scatter.1
where the time goes:
time: 93.2 us; the launch traced here: 92.6 us
  waiting for transfers between devices  58.4 us (63%)
  between operations  14.2 us (15%)
  matrix products  8.2 us (9%)
  other arithmetic  6.98 us (7%)
  local copies, waits for them, and re-layouts  4.67 us (5%)
    all_gather x1, waiting for transfers between devices, on_device(): lax.all_gather(out_weight, 'kv', axis=1, tiled=True)  42.7 us
    reduce_scatter x1, waiting for transfers between devices, on_device(): lax.psum_scatter(terms, 'tp', scatter_dimension=1, tiled=True)  15 us
    unnamed x17, local copies, waits for them, and re-layouts  3.9 us
    dot_general x1, matrix products, on_device(): jnp.einsum('spr,rc->spc', hidden, lax.all_gather(out_weight, 'kv', axis=1...  2.77 us
    dot_general x1, matrix products, cell(): jnp.einsum('hld,hle->hde', g_tok[..., None] * keys, values, precision=HIGH)  2.7 us
  transfers between devices with their start and end apart: 2, of which 2 were waited for; matrix products, arithmetic and copies ran while one was open for 17% of the time, Pallas kernels for 0%

commit v1 on v0

--- a/solution.py
+++ b/solution.py
@@ -4,6 +4,14 @@
 from jax.sharding import PartitionSpec as P
 
 HIGH = lax.Precision.HIGHEST
+
+
+def direct_stacks_all_on(frame, axis_no):
+    frame = jnp.moveaxis(frame, 0, axis_no)
+    seen_now = frame.shape
+    return frame.reshape(
+        *seen_now[:axis_no], seen_now[axis_no] * seen_now[axis_no + 1], *seen_now[axis_no + 2 :]
+    )
 
 
 def cell(queries, keys, values, in_gates, log_forget, memory, normal, stab):
@@ -118,11 +126,28 @@
         state_max,
         norm_gain,
     )
-    terms = jnp.einsum(
-        "spr,rc->spc",
-        hidden,
-        lax.all_gather(out_weight, "kv", axis=1, tiled=True),
-        preferred_element_type=jnp.float32,
+
+    def name_ways(u_in, peer_axis, array_axis, inputs, join_dim):
+        built = lax.axis_size(peer_axis)
+        o_now, v_next, reply = (built, lax.axis_index(peer_axis), u_in.shape[array_axis])
+        pages = []
+        pieces_in = tuple(((i0, (i0 + 1) % o_now) for i0 in range(o_now)))
+        f_next = u_in
+        for t in tuple(range(o_now)):
+            side_arr = f_next if t == o_now - 1 else lax.ppermute(f_next, peer_axis, perm=pieces_in)
+            pages.append(inputs(f_next, (v_next - t) % o_now * reply))
+            f_next = side_arr
+        pages = jnp.stack(pages, 0)[(v_next - jnp.arange(o_now)) % o_now]
+        return direct_stacks_all_on(pages, join_dim)
+
+    terms = name_ways(
+        out_weight,
+        "kv",
+        1,
+        lambda own_block, start: jnp.einsum(
+            "spr,rc->spc", hidden, own_block, preferred_element_type=jnp.float32
+        ),
+        2,
     )
     mixed = lax.psum_scatter(terms, "tp", scatter_dimension=1, tiled=True).astype(jnp.bfloat16)
     return (mixed, new_mem, new_norm, new_max)

time: 93.2 us -> 109 us (1.17)
  waiting for transfers between devices: 58.4 us -> 66.3 us
  starting transfers between devices: 0.08 us -> 4.67 us
  matrix products: 8.2 us -> 10.1 us
  local copies, waits for them, and re-layouts: 4.67 us -> 5.95 us
    ppermute x0 -> x7, waiting for transfers between devices: none -> 52.1 us  [name_ways(): lax.ppermute(f_next, peer_axis, perm=pieces_in)]
    all_gather x1 -> x0, waiting for transfers between devices: 42.7 us -> none  [on_device(): lax.all_gather(out_weight, 'kv', axis=1, tiled=True)]
    ppermute x0 -> x7, starting transfers between devices: none -> 4.63 us  [name_ways(): lax.ppermute(f_next, peer_axis, perm=pieces_in)]
    dot_general x1, matrix products: 1.11 us -> 2.69 us  [cell(): jnp.einsum('hld,hde->hle', queries, memory, precision=HIGH)]
    dot_general x1 -> x8, matrix products: 2.77 us -> 3.11 us  [on_device(): jnp.einsum('spr,rc->spc', hidden, own_block, preferred_element_type=jnp.f...]
    unnamed x17 -> x19, local copies, waits for them, and re-layouts: 3.9 us -> 3.9 us
  transfers between devices with their start and end apart: 2 -> 8, of which waited for: 2 -> 7; matrix products, arithmetic and copies ran while one was open for 17% -> 19% of each run, Pallas kernels for 0% -> 0%
where the time goes in v1:
time: 109 us; the launch traced here: 108 us
  waiting for transfers between devices  66.3 us (61%)
  between operations  14.3 us (13%)
  matrix products  10.1 us (9%)
  other arithmetic  7.01 us (6%)
  local copies, waits for them, and re-layouts  5.95 us (5%)
  starting transfers between devices  4.67 us (4%)
    ppermute x7, waiting for transfers between devices, name_ways(): lax.ppermute(f_next, peer_axis, perm=pieces_in)  52.1 us
    reduce_scatter x1, waiting for transfers between devices, on_device(): lax.psum_scatter(terms, 'tp', scatter_dimension=1, tiled=True)  14.1 us
    ppermute x7, starting transfers between devices, name_ways(): lax.ppermute(f_next, peer_axis, perm=pieces_in)  4.63 us
    unnamed x19, local copies, waits for them, and re-layouts  3.9 us
    dot_general x8, matrix products, on_device(): jnp.einsum('spr,rc->spc', hidden, own_block, preferred_element_type=jnp.f...  3.11 us
    dot_general x1, matrix products, cell(): jnp.einsum('hld,hde->hle', queries, memory, precision=HIGH)  2.69 us
    dot_general x1, matrix products, cell(): jnp.einsum('hld,hle->hde', g_tok[..., None] * keys, values, precision=HIGH)  2.69 us
  transfers between devices with their start and end apart: 8, of which 7 were waited for; matrix products, arithmetic and copies ran while one was open for 19% of the time, Pallas kernels for 0%

profile of v1, /device:TPU:0, one launch (start us, length us, event | category | flops | bytes accessed | tf_op | source)
XLA Modules:
  0.0 108.3 jit_solution(4853809156253745034)
XLA Ops:
  7.2 3.0 %collective-permute-start = (bf16[512,256]{1,0:T(8,128)(2,1)}, bf16[512,256]{1,0:T(8,128)(2,1)S(1)}, u32[]{:S(2)}, u32[]{:S(2)}) collective-permute-start(bf16[512,256]{1,0:T(8,128)(2,1)} %param.29), channel_id=1, source_target_pairs={{0,4},{4,8},{8,12},{12,16},{16,20},{20,24},{24,28},{28,0},{1,5},{5... | collective-permute-start | bytes 786440 | tf_op jit(solution)/shard_map/ppermute | solution.py:137
  10.2 0.7 iota_compare_fusion.1
  10.9 0.7 copy.77
  11.6 0.7 fusion.34
  12.3 0.7 fusion.33
  13.4 0.7 add_maximum_fusion
  14.2 0.7 copy.84
  14.9 0.7 copy.83
  15.7 0.8 copy.88
  16.4 0.8 copy.87
  17.2 0.7 convert_multiply_fusion
  18.0 1.0 fusion.21
  19.0 0.2 fusion.43
  19.3 0.7 fusion.31
  20.3 0.2 fusion.28
  20.5 2.7 %fusion.23 = f32[8,2,8,256]{3,2,1,0:T(8,128)S(1)} fusion(f32[8,2,128,256]{3,2,1,0:T(8,128)} %param.25, f32[8,2,8,128]{3,0,1,2:T(8,128)S(1)} %pad_bitcast_fusion), kind=kOutput, calls=%fused_computation.41 | convolution fusion | flops 50331648 | bytes 2293760 | tf_op jit(solution)/shard_map/vmap(hld,hde->hle)/dot_general | solution.py:28
  23.2 0.3 fusion.25
  23.7 1.6 %collective-permute-start.1 = (bf16[512,256]{1,0:T(8,128)(2,1)S(1)}, bf16[512,256]{1,0:T(8,128)(2,1)S(1)}, u32[]{:S(2)}, u32[]{:S(2)}) collective-permute-start(bf16[512,256]{1,0:T(8,128)(2,1)S(1)} %collective-permute-done), channel_id=1, source_target_pairs={{0,4},{4,8},{8,12},{12,16},{16,20},{20,24},{24,28},{28,0},{1,5},{5... | collective-permute-start | bytes 786440 | tf_op jit(solution)/shard_map/ppermute | solution.py:137
  25.5 8.7 %collective-permute-done.1 = bf16[512,256]{1,0:T(8,128)(2,1)S(1)} collective-permute-done((bf16[512,256]{1,0:T(8,128)(2,1)S(1)}, bf16[512,256]{1,0:T(8,128)(2,1)S(1)}, u32[]{:S(2)}, u32[]{:S(2)}) %collective-permute-start.1) | collective-permute-done | bytes 262176 | tf_op jit(solution)/shard_map/ppermute | solution.py:137
  34.4 9.5 %collective-permute-done.2 = bf16[512,256]{1,0:T(8,128)(2,1)} collective-permute-done((bf16[512,256]{1,0:T(8,128)(2,1)S(1)}, bf16[512,256]{1,0:T(8,128)(2,1)}, u32[]{:S(2)}, u32[]{:S(2)}) %collective-permute-start.2) | collective-permute-done | bytes 262176 | tf_op jit(solution)/shard_map/ppermute | solution.py:137
  44.3 9.0 %collective-permute-done.3 = bf16[512,256]{1,0:T(8,128)(2,1)} collective-permute-done((bf16[512,256]{1,0:T(8,128)(2,1)}, bf16[512,256]{1,0:T(8,128)(2,1)}, u32[]{:S(2)}, u32[]{:S(2)}) %collective-permute-start.3) | collective-permute-done | bytes 262176 | tf_op jit(solution)/shard_map/ppermute | solution.py:137
  53.6 9.0 %collective-permute-done.4 = bf16[512,256]{1,0:T(8,128)(2,1)S(1)} collective-permute-done((bf16[512,256]{1,0:T(8,128)(2,1)}, bf16[512,256]{1,0:T(8,128)(2,1)S(1)}, u32[]{:S(2)}, u32[]{:S(2)}) %collective-permute-start.4) | collective-permute-done | bytes 262176 | tf_op jit(solution)/shard_map/ppermute | solution.py:137
  62.6 1.1 %fusion.4 = f32[8,8,4,256]{3,1,2,0:T(8,128)S(1)} fusion(f32[8,8,4,256]{3,1,2,0:T(8,128)S(1)} %fusion.5, bf16[8,4,512]{2,0,1:T(8,128)(2,1)S(1)} %convert_element_type.20, bf16[512,256]{1,0:T(8,128)(2,1)} %collective-permute-done.2), kind=kOutput, calls=%fused_computation.12 | convolution fusion | flops 8388608 | bytes 327680 | tf_op jit(solution)/shard_map/spr,rc->spc/dot_general | solution.py:147
  63.7 1.1 %fusion.3 = f32[8,8,4,256]{3,1,2,0:T(8,128)S(1)} fusion(f32[8,8,4,256]{3,1,2,0:T(8,128)S(1)} %fusion.4, bf16[8,4,512]{2,0,1:T(8,128)(2,1)S(1)} %convert_element_type.20, bf16[512,256]{1,0:T(8,128)(2,1)} %collective-permute-done.3), kind=kOutput, calls=%fused_computation.10 | convolution fusion | flops 8388608 | bytes 327680 | tf_op jit(solution)/shard_map/spr,rc->spc/dot_general | solution.py:147
  64.8 7.2 %collective-permute-done.5 = bf16[512,256]{1,0:T(8,128)(2,1)S(1)} collective-permute-done((bf16[512,256]{1,0:T(8,128)(2,1)S(1)}, bf16[512,256]{1,0:T(8,128)(2,1)S(1)}, u32[]{:S(2)}, u32[]{:S(2)}) %collective-permute-start.5) | collective-permute-done | bytes 262176 | tf_op jit(solution)/shard_map/ppermute | solution.py:137
  72.3 8.8 %collective-permute-done.6 = bf16[512,256]{1,0:T(8,128)(2,1)S(1)} collective-permute-done((bf16[512,256]{1,0:T(8,128)(2,1)S(1)}, bf16[512,256]{1,0:T(8,128)(2,1)S(1)}, u32[]{:S(2)}, u32[]{:S(2)}) %collective-permute-start.6) | collective-permute-done | bytes 262176 | tf_op jit(solution)/shard_map/ppermute | solution.py:137
  81.2 0.6 gather_fusion
  81.8 0.7 copy.102
  82.5 0.7 multiply_add_fusion.1
  83.2 2.7 %multiply_add_fusion = f32[8,2,128,256]{3,2,1,0:T(8,128)} fusion(f32[8,2,128,256]{3,2,1,0:T(8,128)S(1)} %copy-done, f32[8,2]{1,0:T(8,128)S(1)} %copy.94, bf16[8,4,2,256]{3,1,2,0:T(4,128)(2,1)S(1)} %copy.88, bf16[8,4,2,256]{3,1,2,0:T(4,128)(2,1)S(1)} %copy.87, f32[8,2,8]{2,1,0:T(2,128)S(1)} %copy.95, bf16[8,4,2,128]{3,1,2,0:T(4,128)(2,1)S(1)} %copy.84, ...), kind=kOutput, calls=%fused_computation.1 | convolution fusion | flops 51609600 | bytes 4293184 | tf_op jit(solution)/shard_map/vmap(hld,hle->hde)/dot_general | solution.py:38
  85.9 14.1 %reduce-scatter.2.cloned.1.call-done = f32[8,1,2048]{2,0,1:T(8,128)} async-done(((f32[8,4,2048]{2,0,1:T(8,128)}), f32[8,1,2048]{2,0,1:T(8,128)}) %reduce-scatter.2.cloned.1.call-update) | async-done | bytes 65552 | tf_op jit(solution)/shard_map/reduce_scatter | solution.py:152
  100.0 1.5 %convert_element_type.21 = bf16[8,1,2048]{2,0,1:T(8,128)(2,1)} convert(f32[8,1,2048]{2,0,1:T(8,128)} %reduce-scatter.2.cloned.1.call-done) | non-fusion elementwise | flops 16384 | bytes 98304 | tf_op jit(solution)/shard_map/convert_element_type | solution.py:152
  (56 shorter events, 2.6 us)
Async XLA Ops:
  7.2 92.8 %reduce-scatter.2.cloned.1.call-start = ((), (), s32[]{:S(2)}) async-start(), calls=%async_computation.1 | async-start | bytes 327680 | tf_op jit(solution)/shard_map/reduce_scatter | solution.py:152
  7.2 16.5 %collective-permute-start = (bf16[512,256]{1,0:T(8,128)(2,1)}, bf16[512,256]{1,0:T(8,128)(2,1)S(1)}, u32[]{:S(2)}, u32[]{:S(2)}) collective-permute-start(bf16[512,256]{1,0:T(8,128)(2,1)} %param.29), channel_id=1, source_target_pairs={{0,4},{4,8},{8,12},{12,16},{16,20},{20,24},{24,28},{28,0},{1,5},{5... | collective-permute-start | bytes 786440 | tf_op jit(solution)/shard_map/ppermute | solution.py:137
  14.1 9.5 %copy-start.4 = (f32[8,2,1]{0,2,1:T(1,128)}, f32[8,2,1]{0,2,1:T(1,128)S(1)}, u32[]{:S(2)}) copy-start(f32[8,2,1]{0,2,1:T(1,128)S(1)} %slice.20) | copy-start | bytes 196
  17.9 5.7 %copy-start.3 = (f32[8,2]{0,1:T(2,128)S(1)}, f32[8,2]{0,1:T(2,128)}, u32[]{:S(2)}) copy-start(f32[8,2]{0,1:T(2,128)} %param.27) | copy-start | bytes 196
  17.9 16.3 %copy-start.5 = (f32[2,256]{1,0:T(2,128)S(1)}, f32[2,256]{1,0:T(2,128)}, u32[]{:S(2)}) copy-start(f32[2,256]{1,0:T(2,128)} %param.28) | copy-start | bytes 6148
  19.0 25.2 %copy-start.1 = (bf16[512,256]{1,0:T(8,128)(2,1)S(1)}, bf16[512,256]{1,0:T(8,128)(2,1)}, u32[]{:S(2)}) copy-start(bf16[512,256]{1,0:T(8,128)(2,1)} %param.29) | copy-start | bytes 786436
  23.7 10.5 %collective-permute-start.1 = (bf16[512,256]{1,0:T(8,128)(2,1)S(1)}, bf16[512,256]{1,0:T(8,128)(2,1)S(1)}, u32[]{:S(2)}, u32[]{:S(2)}) collective-permute-start(bf16[512,256]{1,0:T(8,128)(2,1)S(1)} %collective-permute-done), channel_id=1, source_target_pairs={{0,4},{4,8},{8,12},{12,16},{16,20},{20,24},{24,28},{28,0},{1,5},{5... | collective-permute-start | bytes 786440 | tf_op jit(solution)/shard_map/ppermute | solution.py:137
  34.2 9.7 %collective-permute-start.2 = (bf16[512,256]{1,0:T(8,128)(2,1)S(1)}, bf16[512,256]{1,0:T(8,128)(2,1)}, u32[]{:S(2)}, u32[]{:S(2)}) collective-permute-start(bf16[512,256]{1,0:T(8,128)(2,1)S(1)} %collective-permute-done.1), channel_id=1, source_target_pairs={{0,4},{4,8},{8,12},{12,16},{16,20},{20,24},{24,28},{28,0},{1,5},{5... | collective-permute-start | bytes 786440 | tf_op jit(solution)/shard_map/ppermute | solution.py:137
  34.2 48.3 %copy-start.2 = (f32[8,2,128]{2,1,0:T(2,128)S(1)}, f32[8,2,128]{2,1,0:T(2,128)}, u32[]{:S(2)}) copy-start(f32[8,2,128]{2,1,0:T(2,128)} %param.26) | copy-start | bytes 24580
  34.3 48.9 %copy-start = (f32[8,2,128,256]{3,2,1,0:T(8,128)S(1)}, f32[8,2,128,256]{3,2,1,0:T(8,128)}, u32[]{:S(2)}) copy-start(f32[8,2,128,256]{3,2,1,0:T(8,128)} %param.25) | copy-start | bytes 6291460
  43.9 9.4 %collective-permute-start.3 = (bf16[512,256]{1,0:T(8,128)(2,1)}, bf16[512,256]{1,0:T(8,128)(2,1)}, u32[]{:S(2)}, u32[]{:S(2)}) collective-permute-start(bf16[512,256]{1,0:T(8,128)(2,1)} %collective-permute-done.2), channel_id=1, source_target_pairs={{0,4},{4,8},{8,12},{12,16},{16,20},{20,24},{24,28},{28,0},{1,5},{5... | collective-permute-start | bytes 786440 | tf_op jit(solution)/shard_map/ppermute | solution.py:137
  53.3 9.3 %collective-permute-start.4 = (bf16[512,256]{1,0:T(8,128)(2,1)}, bf16[512,256]{1,0:T(8,128)(2,1)S(1)}, u32[]{:S(2)}, u32[]{:S(2)}) collective-permute-start(bf16[512,256]{1,0:T(8,128)(2,1)} %collective-permute-done.3), channel_id=1, source_target_pairs={{0,4},{4,8},{8,12},{12,16},{16,20},{20,24},{24,28},{28,0},{1,5},{5... | collective-permute-start | bytes 786440 | tf_op jit(solution)/shard_map/ppermute | solution.py:137
  62.6 9.4 %collective-permute-start.5 = (bf16[512,256]{1,0:T(8,128)(2,1)S(1)}, bf16[512,256]{1,0:T(8,128)(2,1)S(1)}, u32[]{:S(2)}, u32[]{:S(2)}) collective-permute-start(bf16[512,256]{1,0:T(8,128)(2,1)S(1)} %collective-permute-done.4), channel_id=1, source_target_pairs={{0,4},{4,8},{8,12},{12,16},{16,20},{20,24},{24,28},{28,0},{1,5},{5... | collective-permute-start | bytes 786440 | tf_op jit(solution)/shard_map/ppermute | solution.py:137
  72.0 9.1 %collective-permute-start.6 = (bf16[512,256]{1,0:T(8,128)(2,1)S(1)}, bf16[512,256]{1,0:T(8,128)(2,1)S(1)}, u32[]{:S(2)}, u32[]{:S(2)}) collective-permute-start(bf16[512,256]{1,0:T(8,128)(2,1)S(1)} %collective-permute-done.5), channel_id=1, source_target_pairs={{0,4},{4,8},{8,12},{12,16},{16,20},{20,24},{24,28},{28,0},{1,5},{5... | collective-permute-start | bytes 786440 | tf_op jit(solution)/shard_map/ppermute | solution.py:137
Sparse Core Ops, SparseCore 0:
  82.6 17.3 reduce-scatter.1
